TPU v7x, 32 devices: a whole 2x2x4 slice. The times are simulated.
32 devices in a mesh: ep: 8 (over z, y), tp: 4 (over x, core).
Axes of the slice: x: 2, y: 2, z: 4, core: 2. Of those that a mesh axis runs over, the one named last changes fastest.
Arguments:
- queries: bfloat16 [2048, 1024], P('ep', 'tp'), may hold values from -200 to 200
- keys: bfloat16 [2048, 512], P('ep', 'tp'), may hold values from -5 to 5
- values: bfloat16 [2048, 512], P('ep', 'tp'), may hold values from -6 to 6
- log_gates: float32 [2048, 16], P('ep', 'tp'), may hold values from -2048 to 0, as said below
- out_weight: bfloat16 [1024, 2048], P('tp'), may hold values from -0.1875 to 0.1875
- moe_rows: bfloat16 [2048, 2048], P('ep'), may hold values from -6 to 6
- norm_gain: float32 [2048], replicated, may hold values from 0.1 to 1.9
- experts: int32 [2048, 2], P('ep'), may hold values from 0 to 7, all different within a row; in each aligned block of 256 rows (0 to 255, 256 to 511, ...) at most 128 rows name the same one
- expert_weights: float32 [2048, 2], P('ep'), may hold values from 0.2 to 1
- w_gate: bfloat16 [8, 2048, 1024], P('ep', None, 'tp'), may hold values from -0.125 to 0.125
- w_up: bfloat16 [8, 2048, 1024], P('ep', None, 'tp'), may hold values from -0.125 to 0.125
- w_down: bfloat16 [8, 1024, 2048], P('ep', 'tp'), may hold values from -0.1875 to 0.1875
Outputs:
- mixed: bfloat16 [2048, 2048], P(('ep', 'tp'))
- moe_out: bfloat16 [2048, 2048], P('ep', 'tp')
Inputs may be any that keep to these rules, and one draw needn't show every extreme that they name: Each token names 2 different experts; within the rows of one index of ep (aligned blocks of 256 rows) no expert is named more than 128 times, a bound that some block reaches. `log_gates`: Non-increasing along positions in every head.
All inputs are finite; a program needn't handle non-finite values.
Results may differ from a plain program's by a relative error of at most 0.01195.
Values may be sent and summed in bfloat16 or wider, within the bound.
A program may use at most 128 MiB of HBM per device.

v0:
```python
import math

import jax
import jax.numpy as jnp
from jax import lax
from jax.sharding import PartitionSpec as P

D = 2048
HD = 64


EPSILON = 1e-06
MASKED = -1e30


def prepare_group(query_rows, gate_rows, positions, kv_here, group):
    rows = query_rows.shape[0]
    query_heads = query_rows.reshape(rows, kv_here, group, HD)
    query_gates = jnp.transpose(gate_rows.reshape(rows, kv_here, group), (1, 2, 0))
    return (query_heads, query_gates, positions)


def empty_state(rows, kv_here, group):
    return (
        jnp.full((kv_here, group, rows), MASKED, jnp.float32),
        jnp.zeros((kv_here, group, rows), jnp.float32),
        jnp.zeros((kv_here, group, rows, HD), jnp.float32),
    )


def attend_group(prepared, state, key_part, value_part, gate_part, offset, kv_here, group):
    query_heads, query_gates, query_position = prepared
    length = key_part.shape[0]
    key_span = math.gcd(length, 512)

    def run_blocks(start_state):

        def one_block(turn_index, inner):
            running_max, running_sum, weighted = inner
            first = turn_index * key_span
            key_block = lax.dynamic_slice_in_dim(key_part, first, key_span, 0).reshape(
                key_span, kv_here, HD
            )
            value_block = lax.dynamic_slice_in_dim(value_part, first, key_span, 0).reshape(
                key_span, kv_here, HD
            )
            gate_block = lax.dynamic_slice_in_dim(gate_part, first, key_span, 0).reshape(
                key_span, kv_here, group
            )
            scores = jnp.einsum(
                "qgrd,kgd->grqk", query_heads, key_block, preferred_element_type=jnp.float32
            ) * HD ** (-0.5)
            scores = (
                scores
                + query_gates[..., None]
                - jnp.transpose(gate_block, (1, 2, 0))[:, :, None, :]
            )
            key_position = first + jnp.arange(key_span, dtype=jnp.int32)
            scores = jnp.where(key_position[None, :] <= query_position[:, None], scores, MASKED)
            new_max = jnp.maximum(running_max, jnp.max(scores, axis=-1))
            weights = jnp.exp(scores - new_max[..., None])
            rescale = jnp.exp(running_max - new_max)
            running_sum = running_sum * rescale + jnp.sum(weights, axis=-1)
            weighted = weighted * rescale[..., None] + jnp.einsum(
                "grqk,kgd->grqd",
                weights.astype(jnp.bfloat16),
                value_block,
                preferred_element_type=jnp.float32,
            )
            return (new_max, running_sum, weighted)

        return lax.fori_loop(0, length // key_span, one_block, start_state)

    def keep_state(start_state):
        return start_state

    return lax.cond(offset <= query_position[-1], run_blocks, keep_state, state)


def finish_group(state, heads_here):
    running_max, running_sum, weighted = state
    rows = weighted.shape[2]
    attended = weighted / running_sum[..., None]
    return jnp.transpose(attended, (2, 0, 1, 3)).reshape(rows, heads_here * HD).astype(jnp.bfloat16)


def mixer_half(queries, keys, values, log_gates, out_weight):
    tok_rows = queries.shape[0]
    heads_here = log_gates.shape[1]
    kv_here = keys.shape[1] // HD
    group = heads_here // kv_here
    own_index = lax.axis_index("ep")
    positions = own_index * tok_rows + jnp.arange(tok_rows, dtype=jnp.int32)
    groups = [prepare_group(queries, log_gates, positions, kv_here, group)]
    initial = tuple((empty_state(entry[0].shape[0], kv_here, group) for entry in groups))
    offset = jnp.int32(0)
    key_part = lax.all_gather(keys.astype(jnp.float32), "ep", axis=0, tiled=True).astype(
        jnp.bfloat16
    )
    value_part = lax.all_gather(values.astype(jnp.float32), "ep", axis=0, tiled=True).astype(
        jnp.bfloat16
    )
    gate_part = lax.all_gather(log_gates, "ep", axis=0, tiled=True)
    states = tuple(
        (
            attend_group(
                groups[number],
                initial[number],
                key_part,
                value_part,
                gate_part,
                offset,
                kv_here,
                group,
            )
            for number in range(len(groups))
        )
    )
    finished = [finish_group(state, heads_here) for state in states]
    attended = finished[0]
    return lax.psum_scatter(
        jnp.dot(attended, out_weight, preferred_element_type=jnp.float32).astype(jnp.bfloat16),
        "tp",
        scatter_dimension=0,
        tiled=True,
    )


def experts_half(moe_rows, norm_gain, experts, expert_weights, w_gate, w_up, w_down):
    rows_here = moe_rows.shape[0]
    topk = experts.shape[1]
    experts_all = lax.axis_size("ep")
    capacity = 4 * rows_here // experts_all
    rows_float = moe_rows.astype(jnp.float32)
    normed = (
        rows_float
        * lax.rsqrt(jnp.mean(rows_float * rows_float, axis=-1, keepdims=True) + EPSILON)
        * norm_gain
    ).astype(jnp.bfloat16)
    expert_ids = experts.reshape(-1)
    one_hot = (expert_ids[:, None] == jnp.arange(experts_all, dtype=jnp.int32)[None, :]).astype(
        jnp.int32
    )
    ranks = jnp.cumsum(one_hot, axis=0) - 1
    slot_index = jnp.sum(one_hot * ranks, axis=1)
    destination = expert_ids * capacity + slot_index
    token_index = jnp.arange(rows_here * topk, dtype=jnp.int32) // topk
    width = D // lax.axis_size("tp")
    source_rows = lax.dynamic_slice_in_dim(normed, lax.axis_index("tp") * width, width, 1)
    outgoing = jnp.zeros((experts_all * capacity, source_rows.shape[1]), jnp.bfloat16)
    outgoing = (
        outgoing.at[destination]
        .set(source_rows[token_index])
        .reshape(experts_all, capacity, source_rows.shape[1])
    )
    arrived = lax.all_to_all(outgoing, "ep", split_axis=0, concat_axis=0, tiled=True)
    arrived = lax.all_gather(arrived, "tp", axis=2, tiled=True)
    slots = arrived.shape[1]
    flat_rows = arrived.reshape(-1, D)
    gate_part = jnp.dot(flat_rows, w_gate[0], preferred_element_type=jnp.float32)
    up_part = jnp.dot(flat_rows, w_up[0], preferred_element_type=jnp.float32)
    hidden = (jax.nn.silu(gate_part) * up_part).astype(jnp.bfloat16)
    partial_out = jnp.dot(hidden, w_down[0], preferred_element_type=jnp.float32).reshape(
        experts_all, slots, D
    )
    summed = lax.psum_scatter(
        partial_out.astype(jnp.bfloat16), "tp", scatter_dimension=2, tiled=True
    )
    returned = lax.all_to_all(summed, "ep", split_axis=0, concat_axis=0, tiled=True)
    picked = returned.reshape(experts_all * capacity, -1)[destination].reshape(rows_here, topk, -1)
    return jnp.einsum("tk,tkd->td", expert_weights, picked.astype(jnp.float32)).astype(jnp.bfloat16)


def per_device(
    queries,
    keys,
    values,
    log_gates,
    out_weight,
    moe_rows,
    norm_gain,
    experts,
    expert_weights,
    w_gate,
    w_up,
    w_down,
):
    mixed = mixer_half(queries, keys, values, log_gates, out_weight)
    moe_out = experts_half(moe_rows, norm_gain, experts, expert_weights, w_gate, w_up, w_down)
    return (mixed, moe_out)


def solution(mesh):
    placed = (
        P("ep", "tp"),
        P("ep", "tp"),
        P("ep", "tp"),
        P("ep", "tp"),
        P("tp", None),
        P("ep", None),
        P(),
        P("ep", None),
        P("ep", None),
        P("ep", None, "tp"),
        P("ep", None, "tp"),
        P("ep", "tp", None),
    )
    return jax.shard_map(
        per_device,
        mesh=mesh,
        in_specs=placed,
        out_specs=(P(("ep", "tp"), None), P("ep", "tp")),
        check_vma=False,
    )
```

profile of v0, /device:TPU:0, one launch (start us, length us, event | category | flops | bytes accessed | tf_op | source)
XLA Modules:
  0.0 255.8 jit_solution(16764527390459552446)
XLA Ops:
  7.2 3.0 %convert_element_type.69 = f32[256,2048]{1,0:T(8,128)} convert(bf16[256,2048]{1,0:T(8,128)(2,1)} %param.21) | non-fusion elementwise | flops 524288 | bytes 3145728 | tf_op jit(solution)/shard_map/convert_element_type | solution.py:134
  14.7 5.0 %scatter_custom_fusion = bf16[1024,512]{1,0:T(8,128)(2,1)S(1)} fusion(s32[512]{0:T(512)S(1)} %bitcast.85, bf16[256,512]{1,0:T(8,128)(2,1)S(1)} %fusion.14, s32[1024]{0:T(1024)S(1)} %pad_clamp_fusion.1, bf16[]{:T(256)} %constant.107.clone.1), kind=kCustom, calls=%fused_computation.35 | custom fusion | bytes 1048578 | tf_op jit(solution)/shard_map/scatter | solution.py:153
  19.8 33.0 %all_to_all.10 = bf16[8,128,512]{2,1,0:T(8,128)(2,1)} all-to-all(bf16[8,128,512]{2,1,0:T(8,128)(2,1)S(1)} %bitcast.78), channel_id=1, replica_groups=mesh['ep'=8,'tp'=4] {'ep'}, dimensions={0} | all-to-all | bytes 2097152 | tf_op jit(solution)/shard_map/all_to_all | solution.py:156
  52.9 33.6 %all-gather.2.cloned.1.call-done = bf16[8,128,2048]{2,1,0:T(8,128)(2,1)} async-done(((bf16[8,128,512]{2,1,0:T(8,128)(2,1)}), bf16[8,128,2048]{2,1,0:T(8,128)(2,1)}) %all-gather.2.cloned.1.call-update) | async-done | bytes 4194320 | tf_op jit(solution)/shard_map/all_gather | solution.py:157
  86.4 3.6 %fusion.11 = f32[1024,256]{1,0:T(8,128)S(1)} fusion(bf16[1024,2048]{1,0:T(8,128)(2,1)} %bitcast.91, bf16[1,2048,256]{2,1,0:T(8,128)(2,1)S(1)} %copy-done.9), kind=kOutput, calls=%fused_computation.29 | convolution fusion | flops 1073741824 | bytes 6291456 | tf_op jit(solution)/shard_map/dot_general | solution.py:160
  91.5 3.2 %convolution_convert_fusion = bf16[8,128,2048]{2,1,0:T(8,128)(2,1)} fusion(bf16[8,128,256]{2,1,0:T(8,128)(2,1)S(1)} %bitcast.81, bf16[1,256,2048]{2,1,0:T(8,128)(2,1)S(1)} %copy-done), kind=kOutput, calls=%fused_computation.22 | convolution fusion | flops 1075838976 | bytes 5767168 | tf_op jit(solution)/shard_map/dot_general | solution.py:163
  97.0 30.7 %all_gather.13 = f32[2048,4]{0,1:T(4,128)S(1)} all-gather(f32[256,4]{0,1:T(4,128)S(1)} %copy-done.5), channel_id=1, replica_groups=mesh['ep'=8,'tp'=4] {'ep'}, dimensions={0}, use_global_device_ids=true | all-gather | bytes 36864 | tf_op jit(solution)/shard_map/all_gather | solution.py:103
  127.7 33.5 %all_gather.12 = bf16[2048,128]{0,1:T(8,128)(2,1)} all-gather(bf16[256,128]{0,1:T(8,128)(2,1)S(1)} %copy.20), channel_id=1, replica_groups=mesh['ep'=8,'tp'=4] {'ep'}, dimensions={0}, use_global_device_ids=true | all-gather | bytes 589824 | tf_op jit(solution)/shard_map/all_gather | solution.py:97
  161.2 33.4 %all_gather.14 = bf16[2048,128]{0,1:T(8,128)(2,1)} all-gather(bf16[256,128]{0,1:T(8,128)(2,1)S(1)} %copy.21), channel_id=1, replica_groups=mesh['ep'=8,'tp'=4] {'ep'}, dimensions={0}, use_global_device_ids=true | all-gather | bytes 589824 | tf_op jit(solution)/shard_map/all_gather | solution.py:100
  194.5 25.2 %conditional.1 = (f32[2,2,256]{2,1,0:T(2,128)}, f32[2,2,256,64]{2,3,1,0:T(8,128)}) conditional(s32[]{:T(128)} %bitcast.1, () %tuple.30, (bf16[256,256]{1,0:T(8,128)(2,1)S(1)}, s32[256]{0:T(256)S(1)}, bf16[2048,128]{0,1:T(8,128)(2,1)}, f32[2,2,256]{2,1,0:T(2,128)S(1)}, f32[2048,4]{0,1:T(4,128)S(1)}, /*index=5*/bf16[2048,128]{0,1:T(8,128)(2,1)}) %tuple.69), branch_computations={%region_0.0_spmd, %region_1.6_spmd} | conditional | flops 139269632 | bytes 8373587 | solution.py:77
  195.3 24.4 %while.17 = (s32[]{:T(128)}, f32[2,2,256]{2,1,0:T(2,128)S(1)}, f32[2,2,256]{2,1,0:T(2,128)}, f32[2,2,256,64]{2,3,1,0:T(8,128)}, s32[256]{0:T(256)S(1)}, /*index=...) while((s32[]{:T(128)}, f32[2,2,256]{2,1,0:T(2,128)S(1)}, ...), condition=%wide.region_5.5_spmd.clone, body=%wide.region_2.4_spmd.clone.sunk | while | flops 139269632 | bytes 8111307 | solution.py:72
  196.5 1.6 fusion.44
  201.4 1.6 fusion.44
  203.3 1.3 fusion.47
  204.6 2.1 convolution_add_fusion.2
  207.9 1.6 fusion.44
  209.8 1.3 fusion.47
  211.1 2.1 convolution_add_fusion.2
  214.4 1.6 fusion.44
  217.6 2.1 convolution_add_fusion.2
  220.7 2.7 %convolution_convert_fusion.1 = bf16[256,2048]{1,0:T(8,128)(2,1)} fusion(bf16[256,256]{0,1:T(8,128)(2,1)S(1)} %bitcast.80, bf16[256,2048]{1,0:T(8,128)(2,1)} %param.20), kind=kOutput, calls=%fused_computation.23 | convolution fusion | flops 268959744 | bytes 2228224 | tf_op jit(solution)/shard_map/dot_general | solution.py:122
  223.5 5.8 %all-to-all-start.1 = ((bf16[8,128,512]{2,1,0:T(8,128)(2,1)}), bf16[8,128,512]{2,1,0:T(8,128)(2,1)S(1)}, u32[]{:S(2)}, u32[]{:S(2)}) async-start(bf16[8,128,512]{2,1,0:T(8,128)(2,1)} %reduce-scatter.5.cloned.1.call-done), calls=%async_computation.3 | async-start | bytes 2097152 | tf_op jit(solution)/shard_map/all_to_all | solution.py:169
  229.4 16.2 %all-to-all-done.1 = bf16[8,128,512]{2,1,0:T(8,128)(2,1)S(1)} async-done(((bf16[8,128,512]{2,1,0:T(8,128)(2,1)}), bf16[8,128,512]{2,1,0:T(8,128)(2,1)S(1)}, u32[]{:S(2)}, u32[]{:S(2)}) %all-to-all-start.1) | async-done | bytes 1048608 | tf_op jit(solution)/shard_map/all_to_all | solution.py:169
  245.6 2.0 gather_fusion
  (100 shorter events, 20.1 us)
Async XLA Ops:
  7.2 84.3 %copy-start = (bf16[1,256,2048]{2,1,0:T(8,128)(2,1)S(1)}, bf16[1,256,2048]{2,1,0:T(8,128)(2,1)}, u32[]{:S(2)}) copy-start(bf16[1,256,2048]{2,1,0:T(8,128)(2,1)} %param.27) | copy-start | bytes 3145732
  7.2 3.0 %copy-start.1 = (bf16[256,2048]{1,0:T(8,128)(2,1)S(1)}, bf16[256,2048]{1,0:T(8,128)(2,1)}, u32[]{:S(2)}) copy-start(bf16[256,2048]{1,0:T(8,128)(2,1)} %param.21) | copy-start | bytes 3145732
  7.2 79.2 %all-gather.2.cloned.1.call-start = ((), (), s32[]{:S(2)}) async-start(), calls=%async_computation.5 | async-start | bytes 5242880 | tf_op jit(solution)/shard_map/all_gather | solution.py:157
  7.2 3.3 %copy-start.6 = (s32[256,2]{0,1:T(2,128)S(1)}, s32[256,2]{0,1:T(2,128)}, u32[]{:S(2)}) copy-start(s32[256,2]{0,1:T(2,128)} %param.23) | copy-start | bytes 6148
  14.7 71.7 %copy-start.9 = (bf16[1,2048,256]{2,1,0:T(8,128)(2,1)S(1)}, bf16[1,2048,256]{2,1,0:T(8,128)(2,1)}, u32[]{:S(2)}) copy-start(bf16[1,2048,256]{2,1,0:T(8,128)(2,1)} %param.25) | copy-start | bytes 3145732
  52.8 170.7 %reduce-scatter.5.cloned.1.call-start = ((), (), s32[]{:S(2)}) async-start(), calls=%async_computation.6 | async-start | bytes 5242880 | tf_op jit(solution)/shard_map/reduce_scatter | solution.py:166
  86.4 3.6 %copy-start.8 = (bf16[8,128,2048]{2,1,0:T(8,128)(2,1)S(1)}, bf16[8,128,2048]{2,1,0:T(8,128)(2,1)}, u32[]{:S(2)}) copy-start(bf16[8,128,2048]{2,1,0:T(8,128)(2,1)} %all-gather.2.cloned.1.call-done) | copy-start | bytes 12582916
  86.4 3.7 %copy-start.10 = (bf16[1,2048,256]{2,1,0:T(8,128)(2,1)S(1)}, bf16[1,2048,256]{2,1,0:T(8,128)(2,1)}, u32[]{:S(2)}) copy-start(bf16[1,2048,256]{2,1,0:T(8,128)(2,1)} %param.26) | copy-start | bytes 3145732
  94.7 0.8 copy-start.3
  94.7 1.0 copy-start.4
  94.7 1.1 copy-start.5
  94.7 99.9 %copy-start.2 = (bf16[256,256]{1,0:T(8,128)(2,1)S(1)}, bf16[256,256]{1,0:T(8,128)(2,1)}, u32[]{:S(2)}) copy-start(bf16[256,256]{1,0:T(8,128)(2,1)} %param.16) | copy-start | bytes 393220
  94.7 154.6 %reduce-scatter.3.cloned.1.call-start = ((), (), s32[]{:S(2)}) async-start(), calls=%async_computation.4 | async-start | bytes 1310720 | tf_op jit(solution)/shard_map/reduce_scatter | solution.py:121
  223.4 5.8 %copy-start.7 = (f32[256,2]{0,1:T(2,128)S(1)}, f32[256,2]{0,1:T(2,128)}, u32[]{:S(2)}) copy-start(f32[256,2]{0,1:T(2,128)} %param.24) | copy-start | bytes 6148
  223.5 22.2 %all-to-all-start.1 = ((bf16[8,128,512]{2,1,0:T(8,128)(2,1)}), bf16[8,128,512]{2,1,0:T(8,128)(2,1)S(1)}, u32[]{:S(2)}, u32[]{:S(2)}) async-start(bf16[8,128,512]{2,1,0:T(8,128)(2,1)} %reduce-scatter.5.cloned.1.call-done), calls=%async_computation.3 | async-start | bytes 2097152 | tf_op jit(solution)/shard_map/all_to_all | solution.py:169
Sparse Core Ops, SparseCore 0:
  52.9 33.4 all-gather.1
  94.8 44.3 reduce-scatter.4
  223.6 25.0 reduce-scatter.2
where the time goes:
time: 257 us; the launch traced here: 256 us
  blocking collectives  131 us (51%)
  waiting for transfers between devices  49.8 us (19%)
  matrix products  25.3 us (10%)
  local copies, waits for them, and re-layouts  16.4 us (6%)
  between operations  14.7 us (6%)
  other arithmetic  13 us (5%)
  starting transfers between devices  5.88 us (2%)
    all_gather x1, waiting for transfers between devices, experts_half(): arrived = lax.all_gather(arrived, 'tp', axis=2, tiled=True)  33.6 us
    all_gather x1, blocking collectives, mixer_half(): lax.all_gather(keys.astype(jnp.float32), 'ep', axis=0, tiled=True)  33.5 us
    all_gather x1, blocking collectives, mixer_half(): lax.all_gather(values.astype(jnp.float32), 'ep', axis=0, tiled=True)  33.4 us
    all_to_all x1, blocking collectives, experts_half(): lax.all_to_all(outgoing, 'ep', split_axis=0, concat_axis=0, tiled=True)  33 us
    all_gather x1, blocking collectives, mixer_half(): gate_part = lax.all_gather(log_gates, 'ep', axis=0, tiled=True)  30.7 us
    all_to_all x1, waiting for transfers between devices, experts_half(): lax.all_to_all(summed, 'ep', split_axis=0, concat_axis=0, tiled=True)  16.2 us
    dot_general x4, matrix products, one_block(): jnp.einsum('grqk,kgd->grqd', weights.astype(jnp.bfloat16), value_block, p...  7.5 us
    dot_general x4, matrix products, one_block(): jnp.einsum('qgrd,kgd->grqk', query_heads, key_block, preferred_element_ty...  6.37 us
  transfers between devices with their start and end apart: 4, of which 2 were waited for; matrix products, arithmetic and copies ran while one was open for 13% of the time, Pallas kernels for 0%

commit v1 on v0

--- a/solution.py
+++ b/solution.py
@@ -1,8 +1,11 @@
+import functools
 import math
 
 import jax
 import jax.numpy as jnp
 from jax import lax
+from jax.experimental import pallas as pl
+from jax.experimental.pallas import tpu as pltpu
 from jax.sharding import PartitionSpec as P
 
 D = 2048
@@ -171,6 +174,560 @@
     return jnp.einsum("tk,tkd->td", expert_weights, picked.astype(jnp.float32)).astype(jnp.bfloat16)
 
 
+MESH = pl.DeviceIdType.MESH
+VMEM_BUDGET = 56 * 2**20
+
+
+def fits_fused(keys, log_gates, moe_rows, w_gate, experts):
+    n_ep, n_tp = lax.axis_size("ep"), lax.axis_size("tp")
+    rows_here, width = moe_rows.shape
+    slots = n_ep * (4 * rows_here // n_ep)
+    moved = 2 * (4 * slots * width + 3 * math.prod(w_gate.shape) + 8 * rows_here * width)
+    return (
+        n_tp == 4
+        and n_ep == 8
+        and w_gate.shape[0] == 1
+        and experts.shape[1] == 2
+        and 2 * keys.shape[1] == rows_here
+        and 3 * log_gates.shape[1] <= 16
+        and moved < VMEM_BUDGET
+    )
+
+
+def fused_kernel(
+    n_ep,
+    cap,
+    kv_here,
+    group,
+    q_ref,
+    blk_ref,
+    qgate_ref,
+    rows_ref,
+    gain_ref,
+    ext_ref,
+    ex_ref,
+    ew_ref,
+    wo_hbm,
+    wg_hbm,
+    wu_hbm,
+    wd_hbm,
+    mixed_ref,
+    moe_ref,
+    wo,
+    wg,
+    wu,
+    wd,
+    nbuf,
+    stage,
+    buf,
+    pbuf,
+    in1,
+    qown,
+    qsend,
+    in2,
+    tot,
+    ret,
+    kv,
+    att,
+    mpart,
+    min1,
+    mq,
+    min2,
+    wsem,
+    s_disp,
+    r_disp,
+    s_kv,
+    r_kv,
+    s_rs,
+    r_rs,
+    s_ret,
+    r_ret,
+    s_mix,
+    r_mix,
+):
+    e = lax.axis_index("ep")
+    j = lax.axis_index("tp")
+    zs = n_ep // 2
+    z, y = e // 2, e % 2
+    mate = j + 1 - 2 * (j % 2)
+    across = (j + 2) % 4
+    diag = (mate + 2) % 4
+    y_mate = 2 * z + 1 - y
+    tok = rows_ref.shape[0]
+    quarter = rows_ref.shape[1] // 4
+    f32, bf16 = jnp.float32, jnp.bfloat16
+
+    def remote(source, target, send, recv, to_ep, to_tp):
+        return pltpu.make_async_remote_copy(
+            src_ref=source,
+            dst_ref=target,
+            send_sem=send,
+            recv_sem=recv,
+            device_id=(to_ep, to_tp),
+            device_id_type=MESH,
+        )
+
+    barrier = pltpu.get_barrier_semaphore()
+    for d in range(1, n_ep):
+        pl.semaphore_signal(barrier, inc=1, device_id=((e + d) % n_ep, j), device_id_type=MESH)
+    for other in (mate, across):
+        pl.semaphore_signal(barrier, inc=1, device_id=(e, other), device_id_type=MESH)
+    weight_copies = [
+        pltpu.make_async_copy(a, b, wsem.at[i])
+        for i, (a, b) in enumerate(((wg_hbm, wg), (wu_hbm, wu), (wd_hbm, wd), (wo_hbm, wo)))
+    ]
+    for copy in weight_copies:
+        copy.start()
+
+    kv[e] = blk_ref[...]
+    rows_float = rows_ref[...].astype(f32)
+    scale = lax.rsqrt(jnp.mean(rows_float * rows_float, axis=-1, keepdims=True) + EPSILON)
+    nbuf[...] = (rows_float * scale * gain_ref[...]).astype(bf16)
+
+    row_i = lax.broadcasted_iota(jnp.int32, (tok, tok), 0)
+    col_i = lax.broadcasted_iota(jnp.int32, (tok, tok), 1)
+    upper = jnp.where(row_i < col_i, 1.0, 0.0).astype(bf16)
+    lower = jnp.where(col_i < row_i, 1.0, 0.0).astype(bf16)
+    names_t = lax.broadcasted_iota(jnp.int32, (n_ep, tok), 0)
+    chosen_t = jnp.where(
+        (names_t == ext_ref[0:1, :]) | (names_t == ext_ref[1:2, :]), 1.0, 0.0
+    )
+    rank_t = jnp.dot(chosen_t.astype(bf16), upper, preferred_element_type=f32)
+    key_t = jnp.where(chosen_t > 0.5, rank_t, -1.0)
+    slot_rows = lax.broadcasted_iota(jnp.int32, (cap, tok), 0).astype(f32)
+
+    def pick(expert):
+        line = jnp.sum(jnp.where(names_t == expert, key_t, 0.0), axis=0, keepdims=True)
+        return jnp.where(slot_rows == line, 1.0, 0.0).astype(bf16)
+
+    def slot(d):
+        return pl.ds(d * cap, cap)
+
+    pl.semaphore_wait(barrier, n_ep + 1)
+
+    def kv_line(i):
+        block = e - 2 * i
+        return remote(
+            kv.at[block], kv.at[block], s_kv.at[0, i], r_kv.at[0, i + 1], e + 2, j
+        )
+
+    def kv_side(i):
+        block = e - 2 * i
+        return remote(kv.at[block], kv.at[block], s_kv.at[1, i], r_kv.at[1, i], y_mate, j)
+
+    def kv_line_arrival(i):
+        block = e - 2 * i
+        return remote(
+            kv.at[block], kv.at[block], s_kv.at[0, i], r_kv.at[0, i], y_mate, j
+        )
+
+    def kv_step(i):
+        if i == 0:
+
+            @pl.when(z + 1 < zs)
+            def _():
+                kv_line(0).start()
+
+            @pl.when(y == 0)
+            def _():
+                kv_side(0).start()
+
+            return
+
+        @pl.when(z >= i)
+        def _():
+            kv_line_arrival(i).wait_recv()
+
+            @pl.when(z + 1 < zs)
+            def _():
+                kv_line(i).start()
+
+            kv_side(i).start()
+
+    def kv_finish():
+        @pl.when(y == 1)
+        def _():
+            block = e - 1
+            remote(
+                kv.at[block], kv.at[block], s_kv.at[1, 0], r_kv.at[1, 0], y_mate, j
+            ).wait_recv()
+
+        for i in range(1, zs):
+
+            @pl.when(z >= i)
+            def _():
+                block = 2 * (z - i) + 1 - y
+                remote(
+                    kv.at[block], kv.at[block], s_kv.at[1, i], r_kv.at[1, i], y_mate, j
+                ).wait_recv()
+
+    def kv_drain():
+        for i in range(zs):
+
+            @pl.when((z >= i) & (z + 1 < zs))
+            def _():
+                kv_line(i).wait_send()
+
+            if i == 0:
+
+                @pl.when(y == 0)
+                def _():
+                    kv_side(0).wait_send()
+            else:
+
+                @pl.when(z >= i)
+                def _():
+                    kv_side(i).wait_send()
+
+    kv_step(0)
+
+    own_columns = pl.ds(pl.multiple_of(j * quarter, quarter), quarter)
+    first = {}
+    for d in range(1, n_ep):
+        to = (e + d) % n_ep
+        stage[d - 1] = jnp.dot(
+            pick(to), nbuf[:, own_columns], preferred_element_type=f32
+        ).astype(bf16)
+        first[d] = remote(
+            stage.at[d - 1], buf.at[j, slot(d)], s_disp.at[0, d], r_disp.at[0, d], to, j
+        )
+        first[d].start()
+    own_pick = pick(e)
+    for part in range(4):
+        buf[part, 0:cap, :] = jnp.dot(
+            own_pick, nbuf[:, part * quarter : (part + 1) * quarter], preferred_element_type=f32
+        ).astype(bf16)
+    for copy in weight_copies:
+        copy.wait()
+
+    def spread(kind, part, d, to_tp):
+        return remote(
+            buf.at[part, slot(d)],
+            buf.at[part, slot(d)],
+            s_disp.at[kind, d],
+            r_disp.at[kind, d],
+            e,
+            to_tp,
+        )
+
+    def arrive(d):
+        first[d].wait_recv()
+        spread(2, j, d, across).start()
+        spread(1, j, d, mate).start()
+
+    def relay(d):
+        spread(2, across, d, across).wait_recv()
+        spread(3, across, d, mate).start()
+
+    def ready(d):
+        if d:
+            spread(1, mate, d, mate).wait_recv()
+            spread(3, diag, d, mate).wait_recv()
+
+    span = 2 * cap
+
+    def rs_send(g):
+        rows = pl.ds(g * span, span)
+        return (
+            remote(pbuf.at[mate, rows], in1.at[0, rows], s_rs.at[0, g], r_rs.at[0, g], e, mate),
+            remote(pbuf.at[diag, rows], in1.at[1, rows], s_rs.at[1, g], r_rs.at[1, g], e, mate),
+        )
+
+    def rs_cross(g):
+        rows = pl.ds(g * span, span)
+        return remote(qsend.at[rows], in2.at[rows], s_rs.at[2, g], r_rs.at[2, g], e, across)
+
+    def send_back(d):
+        return remote(
+            tot.at[slot(d)], ret.at[slot(d)], s_ret.at[d], r_ret.at[d], (e + n_ep - d) % n_ep, j
+        )
+
+    def compute(g):
+        ready(2 * g)
+        ready(2 * g + 1)
+        rows = slice(g * span, (g + 1) * span)
+        gate = jnp.zeros((span, wg.shape[1]), f32)
+        up = jnp.zeros((span, wg.shape[1]), f32)
+        for part in range(4):
+            block = buf[part, rows, :]
+            deep = slice(part * quarter, (part + 1) * quarter)
+            gate = gate + jnp.dot(block, wg[deep, :], preferred_element_type=f32)
+            up = up + jnp.dot(block, wu[deep, :], preferred_element_type=f32)
+        hidden = (gate / (1.0 + jnp.exp(-gate)) * up).astype(bf16)
+        for part in range(4):
+            pbuf[part, rows, :] = jnp.dot(
+                hidden, wd[:, part * quarter : (part + 1) * quarter], preferred_element_type=f32
+            ).astype(bf16)
+        for copy in reversed(rs_send(g)):
+            copy.start()
+
+    def fold(g):
+        rows = slice(g * span, (g + 1) * span)
+        one, two = rs_send(g)
+        two.wait_recv()
+        qsend[rows, :] = (
+            pbuf[across, rows, :].astype(f32) + in1[1, rows, :].astype(f32)
+        ).astype(bf16)
+        rs_cross(g).start()
+        one.wait_recv()
+
+    def give(g):
+        rows = slice(g * span, (g + 1) * span)
+        rs_cross(g).wait_recv()
+        total = (
+            pbuf[j, rows, :].astype(f32)
+            + in1[0, rows, :].astype(f32)
+            + in2[rows, :].astype(f32)
+        ).astype(bf16)
+        tot[rows, :] = total
+        for d in (2 * g, 2 * g + 1):
+            if d:
+                send_back(d).start()
+
+    heads = kv_here * group
+    hd = HD
+
+    def attend(g):
+        query = jnp.concatenate(
+            [q_ref[:, (g * group + r) * hd : (g * group + r + 1) * hd] for r in range(group)], 0
+        )
+        qg = jnp.concatenate(
+            [qgate_ref[:, g * group + r : g * group + r + 1] for r in range(group)], 0
+        )
+        qrow = jnp.concatenate(
+            [lax.broadcasted_iota(jnp.int32, (tok, tok), 0) for r in range(group)], 0
+        )
+        kcol = lax.broadcasted_iota(jnp.int32, (group * tok, tok), 1)
+
+        def one(b, state):
+            top, total, acc = state
+            k = kv[b, 0:tok, g * hd : (g + 1) * hd]
+            v = kv[b, 0:tok, kv_here * hd + g * hd : kv_here * hd + (g + 1) * hd]
+            gates = kv[b, tok : tok + 16, :].astype(f32)
+            lines = gates[0:heads] + gates[heads : 2 * heads] + gates[2 * heads : 3 * heads]
+            kg = jnp.concatenate(
+                [
+                    jnp.broadcast_to(lines[g * group + r : g * group + r + 1], (tok, tok))
+                    for r in range(group)
+                ],
+                0,
+            )
+            scores = lax.dot_general(
+                query, k, (((1,), (1,)), ((), ())), preferred_element_type=f32
+            ) * (hd**-0.5)
+            scores = scores + qg - kg
+            scores = jnp.where(kcol + (b - e) * tok <= qrow, scores, MASKED)
+            new_top = jnp.maximum(top, jnp.max(scores, axis=-1, keepdims=True))
+            weights = jnp.exp(scores - new_top)
+            rescale = jnp.exp(top - new_top)
+            total = total * rescale + jnp.sum(weights, axis=-1, keepdims=True)
+            acc = acc * rescale + jnp.dot(weights.astype(bf16), v, preferred_element_type=f32)
+            return (new_top, total, acc)
+
+        start = (
+            jnp.full((group * tok, 1), MASKED, f32),
+            jnp.zeros((group * tok, 1), f32),
+            jnp.zeros((group * tok, hd), f32),
+        )
+        _, total, acc = lax.fori_loop(0, e + 1, one, start)
+        out = (acc / total).astype(bf16)
+        pieces = [out[r * tok : (r + 1) * tok] for r in range(group)]
+        att[:, g * group * hd : (g + 1) * group * hd] = jnp.concatenate(pieces, 1)
+
+    part_rows = tok // 4
+
+    def mix_send():
+        return (
+            remote(mpart.at[mate], min1.at[0], s_mix.at[0], r_mix.at[0], e, mate),
+            remote(mpart.at[diag], min1.at[1], s_mix.at[1], r_mix.at[1], e, mate),
+        )
+
+    def mix_cross():
+        return remote(mq, min2, s_mix.at[2], r_mix.at[2], e, across)
+
+    arrive(1)
+    arrive(2)
+    kv_step(1)
+    relay(1)
+    arrive(3)
+    relay(2)
+    compute(0)
+    arrive(4)
+    kv_step(2)
+    relay(3)
+    arrive(5)
+    fold(0)
+    relay(4)
+    compute(1)
+    arrive(6)
+    kv_step(3)
+    relay(5)
+    arrive(7)
+    fold(1)
+    give(0)
+    compute(2)
+    relay(6)
+    relay(7)
+    fold(2)
+    give(1)
+    compute(3)
+    kv_finish()
+    fold(3)
+    attend(0)
+    give(2)
+    attend(1)
+    give(3)
+    partial = jnp.dot(att[...], wo[...], preferred_element_type=f32).astype(bf16)
+    for part in range(4):
+        mpart[part] = partial[part * part_rows : (part + 1) * part_rows]
+    for copy in reversed(mix_send()):
+        copy.start()
+
+    names = lax.broadcasted_iota(jnp.int32, (tok, n_ep), 1)
+    chosen = jnp.where((names == ex_ref[:, 0:1]) | (names == ex_ref[:, 1:2]), 1.0, 0.0)
+    rank = jnp.dot(lower, chosen.astype(bf16), preferred_element_type=f32)
+    weight = jnp.where(names == ex_ref[:, 0:1], ew_ref[:, 0:1], 0.0) + jnp.where(
+        names == ex_ref[:, 1:2], ew_ref[:, 1:2], 0.0
+    )
+    slot_columns = lax.broadcasted_iota(jnp.int32, (tok, cap), 1).astype(f32)
+
+    one, two = mix_send()
+    two.wait_recv()
+    mq[...] = (mpart[across].astype(f32) + min1[1].astype(f32)).astype(bf16)
+    mix_cross().start()
+    one.wait_recv()
+
+    combined = jnp.zeros((tok, quarter), f32)
+    for d in range(n_ep):
+        expert = (e + d) % n_ep
+        mine = names == expert
+        place = jnp.sum(jnp.where(mine, rank, 0.0), axis=1, keepdims=True)
+        factor = jnp.sum(jnp.where(mine, weight, 0.0), axis=1, keepdims=True)
+        spot = jnp.where(slot_columns == place, factor, 0.0)
+        high = spot.astype(bf16)
+        low = (spot - high.astype(f32)).astype(bf16)
+        if d:
+            send_back(d).wait_recv()
+            came = ret[slot(d), :]
+        else:
+            came = tot[slot(0), :]
+        combined = combined + jnp.dot(high, came, preferred_element_type=f32)
+        combined = combined + jnp.dot(low, came, preferred_element_type=f32)
+    moe_ref[...] = combined.astype(bf16)
+
+    mix_cross().wait_recv()
+    mixed_ref[...] = (
+        mpart[j].astype(f32) + min1[0].astype(f32) + min2[...].astype(f32)
+    ).astype(bf16)
+
+    for d in range(1, n_ep):
+        first[d].wait_send()
+        spread(1, j, d, mate).wait_send()
+        spread(2, j, d, across).wait_send()
+        spread(3, across, d, mate).wait_send()
+        send_back(d).wait_send()
+    for g in range(n_ep // 2):
+        for copy in (*rs_send(g), rs_cross(g)):
+            copy.wait_send()
+    for copy in (*mix_send(), mix_cross()):
+        copy.wait_send()
+    kv_drain()
+
+
+def fused_layer(
+    queries,
+    keys,
+    values,
+    log_gates,
+    out_weight,
+    moe_rows,
+    norm_gain,
+    experts,
+    expert_weights,
+    w_gate,
+    w_up,
+    w_down,
+):
+    n_ep = lax.axis_size("ep")
+    tok, width = moe_rows.shape
+    quarter = width // 4
+    cap = 4 * tok // n_ep
+    slots = n_ep * cap
+    kv_here = keys.shape[1] // HD
+    group = log_gates.shape[1] // kv_here
+    bf16, f32 = jnp.bfloat16, jnp.float32
+    lines = log_gates.T
+    high = lax.reduce_precision(lines, 8, 7)
+    left = lines - high
+    middle = lax.reduce_precision(left, 8, 7)
+    gate_rows = jnp.concatenate([high, middle, left - middle], 0).astype(bf16)
+    gate_rows = jnp.pad(gate_rows, ((0, 16 - gate_rows.shape[0]), (0, 0)))
+    block = jnp.concatenate([jnp.concatenate([keys, values], 1), gate_rows], 0)
+    dma, vmem = pltpu.SemaphoreType.DMA, pltpu.VMEM
+    ff = w_gate.shape[2]
+    heads_width = queries.shape[1]
+    vm = pl.BlockSpec(memory_space=pltpu.VMEM)
+    anywhere = pl.BlockSpec(memory_space=pl.ANY)
+    return pl.pallas_call(
+        functools.partial(fused_kernel, n_ep, cap, kv_here, group),
+        out_shape=(
+            jax.ShapeDtypeStruct((tok // 4, width), bf16),
+            jax.ShapeDtypeStruct((tok, quarter), bf16),
+        ),
+        in_specs=[vm] * 8 + [anywhere] * 4,
+        out_specs=(vm, vm),
+        scratch_shapes=[
+            vmem((heads_width, width), bf16),
+            vmem((width, ff), bf16),
+            vmem((width, ff), bf16),
+            vmem((ff, width), bf16),
+            vmem((tok, width), bf16),
+            vmem((n_ep - 1, cap, quarter), bf16),
+            vmem((4, slots, quarter), bf16),
+            vmem((4, slots, quarter), bf16),
+            vmem((2, slots, quarter), bf16),
+            vmem((8, 128), bf16),
+            vmem((slots, quarter), bf16),
+            vmem((slots, quarter), bf16),
+            vmem((slots, quarter), bf16),
+            vmem((slots, quarter), bf16),
+            vmem((n_ep, tok + 16, block.shape[1]), bf16),
+            vmem((tok, heads_width), bf16),
+            vmem((4, tok // 4, width), bf16),
+            vmem((2, tok // 4, width), bf16),
+            vmem((tok // 4, width), bf16),
+            vmem((tok // 4, width), bf16),
+            dma((4,)),
+            dma((4, n_ep)),
+            dma((4, n_ep)),
+            dma((2, n_ep // 2 + 1)),
+            dma((2, n_ep // 2 + 1)),
+            dma((3, n_ep // 2)),
+            dma((3, n_ep // 2)),
+            dma((n_ep,)),
+            dma((n_ep,)),
+            dma((3,)),
+            dma((3,)),
+        ],
+        compiler_params=pltpu.CompilerParams(
+            collective_id=0, has_side_effects=True, vmem_limit_bytes=VMEM_BUDGET
+        ),
+    )(
+        queries,
+        block,
+        log_gates,
+        moe_rows,
+        norm_gain.reshape(1, -1),
+        experts.T,
+        experts,
+        expert_weights,
+        out_weight,
+        w_gate[0],
+        w_up[0],
+        w_down[0],
+    )
+
+
 def per_device(
     queries,
     keys,
@@ -185,6 +742,21 @@
     w_up,
     w_down,
 ):
+    if fits_fused(keys, log_gates, moe_rows, w_gate, experts):
+        return fused_layer(
+            queries,
+            keys,
+            values,
+            log_gates,
+            out_weight,
+            moe_rows,
+            norm_gain,
+            experts,
+            expert_weights,
+            w_gate,
+            w_up,
+            w_down,
+        )
     mixed = mixer_half(queries, keys, values, log_gates, out_weight)
     moe_out = experts_half(moe_rows, norm_gain, experts, expert_weights, w_gate, w_up, w_down)
     return (mixed, moe_out)

time: 257 us -> 95.7 us (0.37)
  blocking collectives: 131 us -> 0 us
  Pallas kernels: 0 us -> 86.6 us
  waiting for transfers between devices: 49.8 us -> 0 us
  matrix products: 25.3 us -> 0 us
  between operations: 14.7 us -> 0.67 us
  other arithmetic: 13 us -> 1.57 us
  local copies, waits for them, and re-layouts: 16.4 us -> 5.49 us
  starting transfers between devices: 5.88 us -> 0 us
    all_gather x3 -> x0, blocking collectives: 97.5 us -> none  [the longest x1 33.5 us: mixer_half(): lax.all_gather(keys.astype(jnp.float32), 'ep', axis=0, tiled=True)]
    pallas_call x0 -> x1, Pallas kernels: none -> 86.6 us  [fused_layer(): pl.pallas_call(functools.partial(fused_kernel, n_ep, cap, kv_here, group)...]
    all_gather x1 -> x0, waiting for transfers between devices: 33.6 us -> none  [experts_half(): arrived = lax.all_gather(arrived, 'tp', axis=2, tiled=True)]
    all_to_all x1 -> x0, blocking collectives: 33 us -> none  [experts_half(): lax.all_to_all(outgoing, 'ep', split_axis=0, concat_axis=0, tiled=True)]
    dot_general x13 -> x0, matrix products: 25.3 us -> none  [the longest x4 7.5 us: one_block(): jnp.einsum('grqk,kgd->grqd', weights.astype(jnp.bfloat16), value_block, p...]
    all_to_all x1 -> x0, waiting for transfers between devices: 16.2 us -> none  [experts_half(): lax.all_to_all(summed, 'ep', split_axis=0, concat_axis=0, tiled=True)]
    all_to_all x1 -> x0, starting transfers between devices: 5.76 us -> none  [experts_half(): lax.all_to_all(summed, 'ep', split_axis=0, concat_axis=0, tiled=True)]
    convert_element_type x4 -> x0, other arithmetic: 5.09 us -> none  [the longest x1 2.96 us: experts_half(): rows_float = moe_rows.astype(jnp.float32)]
  transfers between devices with their start and end apart: 4 -> 0, of which waited for: 2 -> 0; matrix products, arithmetic and copies ran while one was open for 13% -> 0% of each run, Pallas kernels for 0% -> 0%
where the time goes in v1:
time: 95.7 us; the launch traced here: 94.3 us
  Pallas kernels  86.6 us (90%)
  local copies, waits for them, and re-layouts  5.49 us (6%)
  other arithmetic  1.57 us (2%)
    pallas_call x1, Pallas kernels, fused_layer(): pl.pallas_call(functools.partial(fused_kernel, n_ep, cap, kv_here, group)...  86.6 us
    unnamed x13, local copies, waits for them, and re-layouts  5.49 us

profile of v1, /device:TPU:0, one launch (start us, length us, event | category | flops | bytes accessed | tf_op | source)
XLA Modules:
  0.0 94.3 jit_solution(17622528309589697342)
XLA Ops:
  0.6 0.0 copy-start.1
  0.6 0.7 copy-done.1
  1.3 0.0 copy-start.3
  1.4 1.6 %pad_maximum_fusion.blk_ref = bf16[272,256]{1,0:T(8,128)(2,1)} fusion(bf16[16,256]{1,0:T(8,128)(2,1)S(1)} %fusion.4, bf16[256,128]{1,0:T(8,128)(2,1)} %param.14, bf16[256,128]{1,0:T(8,128)(2,1)} %param.13), kind=kLoop, calls=%fused_computation | loop fusion | flops 417792 | bytes 278528 | tf_op jit(solution)/shard_map/concatenate | solution.py:665
  2.9 0.0 copy-done.3
  2.9 0.8 copy.16.ew_ref
  3.7 0.0 copy-start.2
  3.7 0.8 copy.14.qgate_ref
  4.5 0.0 copy-done.2
  4.5 0.8 copy.15.ex_ref
  5.3 86.6 %shard_map.131 = (bf16[64,2048]{1,0:T(8,128)(2,1)}, bf16[256,512]{1,0:T(8,128)(2,1)}) custom-call(bf16[256,256]{1,0:T(8,128)(2,1)} %q_ref.1, bf16[272,256]{1,0:T(8,128)(2,1)} %pad_maximum_fusion.blk_ref, f32[256,4]{1,0:T(8,128)} %copy.14.qgate_ref, bf16[256,2048]{1,0:T(8,128)(2,1)} %rows_ref.1, f32[1,2048]{1,0:T(1,128)} %bitcast.15, s32[2,256]{1,0:T(2,128)} %bitcast.16, ...), custom_call_target="tpu_custom_call" | custom-call | tf_op jit(solution)/shard_map/pallas_call | solution.py:671
  91.9 0.0 copy-start
  91.9 1.7 %copy.19 = bf16[64,2048]{1,0:T(8,128)(2,1)} copy(bf16[64,2048]{1,0:T(8,128)(2,1)} %get-tuple-element.7) | data formatting | bytes 524288
  93.6 0.0 copy-done
  93.6 0.7 copy.20
  (2 shorter events, 0.0 us)
Async XLA Ops:
  0.6 0.7 copy-start.1
  1.3 1.6 %copy-start.3 = (f32[256,2]{0,1:T(2,128)S(1)}, f32[256,2]{0,1:T(2,128)}, u32[]{:S(2)}) copy-start(f32[256,2]{0,1:T(2,128)} %param.20) | copy-start | bytes 6148
  3.7 0.8 copy-start.2
  91.9 1.7 %copy-start = (bf16[256,512]{1,0:T(8,128)(2,1)S(1)}, bf16[256,512]{1,0:T(8,128)(2,1)}, u32[]{:S(2)}) copy-start(bf16[256,512]{1,0:T(8,128)(2,1)} %get-tuple-element.8) | copy-start | bytes 786436

commit v2 on v1

--- a/solution.py
+++ b/solution.py
@@ -189,7 +189,7 @@
         and w_gate.shape[0] == 1
         and experts.shape[1] == 2
         and 2 * keys.shape[1] == rows_here
-        and 3 * log_gates.shape[1] <= 16
+        and log_gates.shape[1] == 4
         and moved < VMEM_BUDGET
     )
 
@@ -200,13 +200,11 @@
     kv_here,
     group,
     q_ref,
-    blk_ref,
-    qgate_ref,
+    k_ref,
+    v_ref,
+    small_ref,
     rows_ref,
     gain_ref,
-    ext_ref,
-    ex_ref,
-    ew_ref,
     wo_hbm,
     wg_hbm,
     wu_hbm,
@@ -228,6 +226,9 @@
     tot,
     ret,
     kv,
+    tops,
+    totals,
+    accs,
     att,
     mpart,
     min1,
@@ -279,7 +280,20 @@
     for copy in weight_copies:
         copy.start()
 
-    kv[e] = blk_ref[...]
+    heads = kv_here * group
+    kv_width = k_ref.shape[1]
+    kv[e, 0:tok, 0:kv_width] = k_ref[...]
+    kv[e, 0:tok, kv_width : 2 * kv_width] = v_ref[...]
+    small = small_ref[...]
+    lines_high = small.astype(bf16).astype(f32)
+    lines_left = small - lines_high
+    lines_mid = lines_left.astype(bf16).astype(f32)
+    kv[e, tok : tok + 32, :] = jnp.concatenate(
+        [lines_high, lines_mid, lines_left - lines_mid, jnp.zeros_like(small)], 0
+    ).astype(bf16)
+    columns = jnp.transpose(small)
+    ex_line = small.astype(jnp.int32)
+    ex_column = columns.astype(jnp.int32)
     rows_float = rows_ref[...].astype(f32)
     scale = lax.rsqrt(jnp.mean(rows_float * rows_float, axis=-1, keepdims=True) + EPSILON)
     nbuf[...] = (rows_float * scale * gain_ref[...]).astype(bf16)
@@ -290,7 +304,7 @@
     lower = jnp.where(col_i < row_i, 1.0, 0.0).astype(bf16)
     names_t = lax.broadcasted_iota(jnp.int32, (n_ep, tok), 0)
     chosen_t = jnp.where(
-        (names_t == ext_ref[0:1, :]) | (names_t == ext_ref[1:2, :]), 1.0, 0.0
+        (names_t == ex_line[heads : heads + 1]) | (names_t == ex_line[heads + 1 : heads + 2]), 1.0, 0.0
     )
     rank_t = jnp.dot(chosen_t.astype(bf16), upper, preferred_element_type=f32)
     key_t = jnp.where(chosen_t > 0.5, rank_t, -1.0)
@@ -344,22 +358,13 @@
 
             kv_side(i).start()
 
-    def kv_finish():
-        @pl.when(y == 1)
+    def side_wait(i):
+        @pl.when((y == 1) if i == 0 else (z >= i))
         def _():
-            block = e - 1
+            block = 2 * (z - i) + 1 - y
             remote(
-                kv.at[block], kv.at[block], s_kv.at[1, 0], r_kv.at[1, 0], y_mate, j
+                kv.at[block], kv.at[block], s_kv.at[1, i], r_kv.at[1, i], y_mate, j
             ).wait_recv()
-
-        for i in range(1, zs):
-
-            @pl.when(z >= i)
-            def _():
-                block = 2 * (z - i) + 1 - y
-                remote(
-                    kv.at[block], kv.at[block], s_kv.at[1, i], r_kv.at[1, i], y_mate, j
-                ).wait_recv()
 
     def kv_drain():
         for i in range(zs):
@@ -397,8 +402,6 @@
         buf[part, 0:cap, :] = jnp.dot(
             own_pick, nbuf[:, part * quarter : (part + 1) * quarter], preferred_element_type=f32
         ).astype(bf16)
-    for copy in weight_copies:
-        copy.wait()
 
     def spread(kind, part, d, to_tp):
         return remote(
@@ -484,55 +487,50 @@
             if d:
                 send_back(d).start()
 
-    heads = kv_here * group
     hd = HD
 
-    def attend(g):
-        query = jnp.concatenate(
-            [q_ref[:, (g * group + r) * hd : (g * group + r + 1) * hd] for r in range(group)], 0
-        )
-        qg = jnp.concatenate(
-            [qgate_ref[:, g * group + r : g * group + r + 1] for r in range(group)], 0
-        )
-        qrow = jnp.concatenate(
-            [lax.broadcasted_iota(jnp.int32, (tok, tok), 0) for r in range(group)], 0
-        )
-        kcol = lax.broadcasted_iota(jnp.int32, (group * tok, tok), 1)
-
-        def one(b, state):
-            top, total, acc = state
-            k = kv[b, 0:tok, g * hd : (g + 1) * hd]
-            v = kv[b, 0:tok, kv_here * hd + g * hd : kv_here * hd + (g + 1) * hd]
-            gates = kv[b, tok : tok + 16, :].astype(f32)
-            lines = gates[0:heads] + gates[heads : 2 * heads] + gates[2 * heads : 3 * heads]
-            kg = jnp.concatenate(
-                [
-                    jnp.broadcast_to(lines[g * group + r : g * group + r + 1], (tok, tok))
-                    for r in range(group)
-                ],
-                0,
-            )
+    def attend(block, own):
+        gates = kv[block, tok : tok + 32, :].astype(f32)
+        lines = gates[0:8] + gates[8:16] + gates[16:24]
+        for h in range(heads):
+            g = h // group
+            query = (q_ref[:, h * hd : (h + 1) * hd].astype(f32) * hd**-0.5).astype(bf16)
+            k = kv[block, 0:tok, g * hd : (g + 1) * hd]
+            v = kv[block, 0:tok, kv_width + g * hd : kv_width + (g + 1) * hd]
             scores = lax.dot_general(
                 query, k, (((1,), (1,)), ((), ())), preferred_element_type=f32
-            ) * (hd**-0.5)
-            scores = scores + qg - kg
-            scores = jnp.where(kcol + (b - e) * tok <= qrow, scores, MASKED)
-            new_top = jnp.maximum(top, jnp.max(scores, axis=-1, keepdims=True))
+            )
+            scores = scores + columns[:, h : h + 1] - lines[h : h + 1]
+            if own:
+                scores = jnp.where(col_i <= row_i, scores, MASKED)
+            new_top = jnp.max(scores, axis=-1, keepdims=True)
+            if not own:
+                new_top = jnp.maximum(tops[h], new_top)
             weights = jnp.exp(scores - new_top)
-            rescale = jnp.exp(top - new_top)
-            total = total * rescale + jnp.sum(weights, axis=-1, keepdims=True)
-            acc = acc * rescale + jnp.dot(weights.astype(bf16), v, preferred_element_type=f32)
-            return (new_top, total, acc)
-
-        start = (
-            jnp.full((group * tok, 1), MASKED, f32),
-            jnp.zeros((group * tok, 1), f32),
-            jnp.zeros((group * tok, hd), f32),
-        )
-        _, total, acc = lax.fori_loop(0, e + 1, one, start)
-        out = (acc / total).astype(bf16)
-        pieces = [out[r * tok : (r + 1) * tok] for r in range(group)]
-        att[:, g * group * hd : (g + 1) * group * hd] = jnp.concatenate(pieces, 1)
+            total = jnp.sum(weights, axis=-1, keepdims=True)
+            acc = jnp.dot(weights.astype(bf16), v, preferred_element_type=f32)
+            if not own:
+                rescale = jnp.exp(tops[h] - new_top)
+                total = total + totals[h] * rescale
+                acc = acc + accs[h] * rescale
+            tops[h] = new_top
+            totals[h] = total
+            accs[h] = acc
+
+    def stage_attention(i):
+        if i == 1:
+            side_wait(0)
+            low, high = 2 * jnp.maximum(z - 1, 0), e
+        else:
+            low = 2 * jnp.maximum(z - i, 0)
+            high = 2 * jnp.maximum(z - i + 1, 0)
+        side_wait(i)
+
+        def one(block, carry):
+            attend(block, False)
+            return carry
+
+        lax.fori_loop(low, high, one, 0)
 
     part_rows = tok // 4
 
@@ -545,12 +543,15 @@
     def mix_cross():
         return remote(mq, min2, s_mix.at[2], r_mix.at[2], e, across)
 
+    attend(e, True)
     arrive(1)
     arrive(2)
     kv_step(1)
     relay(1)
     arrive(3)
     relay(2)
+    for copy in weight_copies:
+        copy.wait()
     compute(0)
     arrive(4)
     kv_step(2)
@@ -562,32 +563,38 @@
     arrive(6)
     kv_step(3)
     relay(5)
+    give(0)
+    stage_attention(1)
     arrive(7)
+    relay(6)
     fold(1)
-    give(0)
+    relay(7)
     compute(2)
-    relay(6)
-    relay(7)
-    fold(2)
     give(1)
     compute(3)
-    kv_finish()
+    fold(2)
+    stage_attention(2)
+    give(2)
     fold(3)
-    attend(0)
-    give(2)
-    attend(1)
-    give(3)
+    stage_attention(3)
+    for h in range(0, heads, 2):
+        att[:, h * hd : (h + 2) * hd] = jnp.concatenate(
+            [accs[h] / totals[h], accs[h + 1] / totals[h + 1]], 1
+        ).astype(bf16)
     partial = jnp.dot(att[...], wo[...], preferred_element_type=f32).astype(bf16)
     for part in range(4):
         mpart[part] = partial[part * part_rows : (part + 1) * part_rows]
     for copy in reversed(mix_send()):
         copy.start()
 
+    give(3)
     names = lax.broadcasted_iota(jnp.int32, (tok, n_ep), 1)
-    chosen = jnp.where((names == ex_ref[:, 0:1]) | (names == ex_ref[:, 1:2]), 1.0, 0.0)
+    first_name, second_name = (ex_column[:, heads + k : heads + k + 1] for k in range(2))
+    first_weight, second_weight = (columns[:, heads + k : heads + k + 1] for k in (2, 3))
+    chosen = jnp.where((names == first_name) | (names == second_name), 1.0, 0.0)
     rank = jnp.dot(lower, chosen.astype(bf16), preferred_element_type=f32)
-    weight = jnp.where(names == ex_ref[:, 0:1], ew_ref[:, 0:1], 0.0) + jnp.where(
-        names == ex_ref[:, 1:2], ew_ref[:, 1:2], 0.0
+    weight = jnp.where(names == first_name, first_weight, 0.0) + jnp.where(
+        names == second_name, second_weight, 0.0
     )
     slot_columns = lax.broadcasted_iota(jnp.int32, (tok, cap), 1).astype(f32)
 
@@ -656,13 +663,7 @@
     kv_here = keys.shape[1] // HD
     group = log_gates.shape[1] // kv_here
     bf16, f32 = jnp.bfloat16, jnp.float32
-    lines = log_gates.T
-    high = lax.reduce_precision(lines, 8, 7)
-    left = lines - high
-    middle = lax.reduce_precision(left, 8, 7)
-    gate_rows = jnp.concatenate([high, middle, left - middle], 0).astype(bf16)
-    gate_rows = jnp.pad(gate_rows, ((0, 16 - gate_rows.shape[0]), (0, 0)))
-    block = jnp.concatenate([jnp.concatenate([keys, values], 1), gate_rows], 0)
+    small = jnp.concatenate([log_gates, experts.astype(f32), expert_weights], 1).T
     dma, vmem = pltpu.SemaphoreType.DMA, pltpu.VMEM
     ff = w_gate.shape[2]
     heads_width = queries.shape[1]
@@ -674,7 +675,7 @@
             jax.ShapeDtypeStruct((tok // 4, width), bf16),
             jax.ShapeDtypeStruct((tok, quarter), bf16),
         ),
-        in_specs=[vm] * 8 + [anywhere] * 4,
+        in_specs=[vm] * 6 + [anywhere] * 4,
         out_specs=(vm, vm),
         scratch_shapes=[
             vmem((heads_width, width), bf16),
@@ -691,7 +692,10 @@
             vmem((slots, quarter), bf16),
             vmem((slots, quarter), bf16),
             vmem((slots, quarter), bf16),
-            vmem((n_ep, tok + 16, block.shape[1]), bf16),
+            vmem((n_ep, tok + 32, tok), bf16),
+            vmem((kv_here * group, tok, 1), f32),
+            vmem((kv_here * group, tok, 1), f32),
+            vmem((kv_here * group, tok, HD), f32),
             vmem((tok, heads_width), bf16),
             vmem((4, tok // 4, width), bf16),
             vmem((2, tok // 4, width), bf16),
@@ -714,13 +718,11 @@
         ),
     )(
         queries,
-        block,
-        log_gates,
+        keys,
+        values,
+        small,
         moe_rows,
         norm_gain.reshape(1, -1),
-        experts.T,
-        experts,
-        expert_weights,
         out_weight,
         w_gate[0],
         w_up[0],

time: 95.7 us -> 94.4 us (0.986); the launches traced: 94.3 us -> 94.1 us
  Pallas kernels: 86.6 us -> 89.1 us
  local copies, waits for them, and re-layouts: 5.49 us -> 3.76 us
  other arithmetic: 1.57 us -> 0.61 us
    pallas_call x1, Pallas kernels: 86.6 us -> 89.1 us  [fused_layer(): pl.pallas_call(functools.partial(fused_kernel, n_ep, cap, kv_here, group)...]
    unnamed x13 -> x10, local copies, waits for them, and re-layouts: 5.49 us -> 3.76 us
    concatenate x2 -> x0, other arithmetic: 1.56 us -> none  [the longest x1 1.55 us: fused_layer(): block = jnp.concatenate([jnp.concatenate([keys, values], 1), gate_rows], 0)]
where the time goes in v2:
time: 94.4 us; the launch traced here: 94.1 us
  Pallas kernels  89.1 us (94%)
  local copies, waits for them, and re-layouts  3.76 us (4%)
    pallas_call x1, Pallas kernels, fused_layer(): pl.pallas_call(functools.partial(fused_kernel, n_ep, cap, kv_here, group)...  89.1 us
    unnamed x10, local copies, waits for them, and re-layouts  3.76 us

profile of v2, /device:TPU:0, one launch (start us, length us, event | category | flops | bytes accessed | tf_op | source)
XLA Modules:
  0.0 94.1 jit_solution(9972902227068666327)
XLA Ops:
  0.6 0.0 copy-start.2
  0.6 0.0 copy-start.1
  0.7 0.7 copy-done.2
  1.3 0.0 copy-start.3
  1.3 0.0 copy-done.1
  1.3 0.7 copy-done.3
  2.0 0.6 maximum_bitcast_fusion.small_ref
  2.6 89.1 %shard_map.131 = (bf16[64,2048]{1,0:T(8,128)(2,1)}, bf16[256,512]{1,0:T(8,128)(2,1)}) custom-call(bf16[256,256]{1,0:T(8,128)(2,1)} %q_ref.1, bf16[256,128]{1,0:T(8,128)(2,1)} %k_ref.1, bf16[256,128]{1,0:T(8,128)(2,1)} %v_ref.1, f32[8,256]{1,0:T(8,128)} %maximum_bitcast_fusion.small_ref, bf16[256,2048]{1,0:T(8,128)(2,1)} %rows_ref.1, f32[1,2048]{1,0:T(1,128)} %bitcast.9, ...), custom_call_target="tpu_custom_call" | custom-call | tf_op jit(solution)/shard_map/pallas_call | solution.py:672
  91.7 0.0 copy-start
  91.7 1.7 %copy.16 = bf16[64,2048]{1,0:T(8,128)(2,1)} copy(bf16[64,2048]{1,0:T(8,128)(2,1)} %get-tuple-element.4) | data formatting | bytes 524288
  93.4 0.0 copy-done
  93.4 0.7 copy.17
  (1 shorter events, 0.0 us)
Async XLA Ops:
  0.6 0.7 copy-start.2
  0.6 0.7 copy-start.1
  1.3 0.7 copy-start.3
  91.7 1.7 %copy-start = (bf16[256,512]{1,0:T(8,128)(2,1)S(1)}, bf16[256,512]{1,0:T(8,128)(2,1)}, u32[]{:S(2)}) copy-start(bf16[256,512]{1,0:T(8,128)(2,1)} %get-tuple-element.5) | copy-start | bytes 786436
